TPU v7x, 32 devices: a whole 2x2x4 slice. The times are simulated.
32 devices in a mesh: ep: 8 (over z, x), tp: 4 (over y, core).
Axes of the slice: x: 2, y: 2, z: 4, core: 2. Of those that a mesh axis runs over, the one named last changes fastest.
Arguments:
- mix_query: bfloat16 [2048, 2048], P('ep', 'tp'), may hold values from -6 to 6
- forget_input: bfloat16 [2048, 2048], P('ep', 'tp'), may hold values from -6 to 6
- mix_value: bfloat16 [2048, 2048], P('ep', 'tp'), may hold values from -6 to 6
- out_gate_input: bfloat16 [2048, 2048], P('ep', 'tp'), may hold values from -6 to 6
- decay_shift: float32 [2048, 16], P('ep', 'tp'), may hold values from -1.5 to 0
- forget_floor: float32 [2048], P('tp'), may hold values from 0.9 to 1
- head_gain: float32 [128], replicated, may hold values from 0.1 to 1.9
- w_mix_out: bfloat16 [2048, 2048], P(None, 'tp'), may hold values from -0.125 to 0.125
- moe_input: bfloat16 [2048, 2048], P('ep'), may hold values from -6 to 6
- moe_gain: float32 [2048], replicated, may hold values from 0.1 to 1.9
- routes: int32 [2048, 2], P('ep'), may hold values from 0 to 7, all different within a row; in each aligned block of 256 rows (0 to 255, 256 to 511, ...) at most 80 rows name the same one
- route_weight: float32 [2048, 2], P('ep'), may hold values from 0.1 to 1
- w_exp_gate: bfloat16 [8, 2048, 4096], P('ep', None, 'tp'), may hold values from -0.125 to 0.125
- w_exp_up: bfloat16 [8, 2048, 4096], P('ep', None, 'tp'), may hold values from -0.125 to 0.125
- w_exp_down: bfloat16 [8, 4096, 2048], P('ep', 'tp'), may hold values from -0.125 to 0.125
Outputs:
- mixed: bfloat16 [2048, 2048], P('ep', 'tp')
- moe_out: bfloat16 [2048, 2048], P('ep', 'tp')
Inputs may be any that keep to these rules, and one draw needn't show every extreme that they name: `routes`: at most 80 of the rows of one index of ep name one expert, and in every draw some device's rows name one expert exactly 80 times; the experts of a row differ.
All inputs are finite; a program needn't handle non-finite values.
Results may differ from a plain program's by a relative error of at most 0.02.
Values may be sent and summed in bfloat16 or wider, within the bound.
A program may use at most 64 MiB of HBM per device.

v0:
```python
import jax
import jax.numpy as jnp
from jax import lax
from jax.sharding import PartitionSpec as P

TOP_K = 2
eps = 1e-06
highest_precision = lax.Precision.HIGHEST


def carried_in(shard, axis, join, neutral):
    place = lax.axis_index(axis)
    gathered = jax.tree.map(
        lambda a, kind: lax.all_gather(a.astype(kind), axis), shard, (jnp.bfloat16, jnp.bfloat16)
    )
    state = jax.tree.map(lambda a, e: jnp.zeros_like(a) + jnp.asarray(e, a.dtype), shard, neutral)

    def one(turn, state):
        return join(
            state,
            jax.tree.map(
                lambda a, own: lax.dynamic_index_in_dim(a, turn, 0, False).astype(own.dtype),
                gathered,
                shard,
            ),
        )

    return lax.fori_loop(0, place, one, state)


def chain_step(earlier, later):
    return (earlier[0] * later[0], later[0][:, :, None] * earlier[1] + later[1])


def token_mixer(
    mix_query,
    forget_input,
    mix_value,
    out_gate_input,
    decay_shift,
    forget_floor,
    head_gain,
    w_mix_out,
):
    length = mix_query.shape[0]
    heads_here = decay_shift.shape[1]
    head_size = head_gain.shape[0]
    gate_input = forget_input.astype(jnp.float32)
    forget = forget_floor + (1.0 - forget_floor) * jax.nn.sigmoid(gate_input)
    input_gate = (1.0 - forget_floor) * jax.nn.sigmoid(-gate_input)
    log_decay = jnp.log(forget) + jnp.repeat(decay_shift, head_size, axis=1)

    def by_head(array):
        return array.reshape(length, heads_here, head_size).transpose(1, 0, 2)

    running_decay = jnp.cumsum(by_head(log_decay), axis=1)
    query_rows = by_head(mix_query.astype(jnp.float32)) * jnp.exp(running_decay)
    head_keys = by_head(input_gate)
    values = by_head(mix_value.astype(jnp.float32))
    scores = jnp.einsum(
        "htk,hsk->hts", query_rows, head_keys * jnp.exp(-running_decay), precision=highest_precision
    )
    causal = jnp.arange(length)[:, None] >= jnp.arange(length)[None, :]
    scores = jnp.where(causal[None, :, :], scores, 0.0)
    within_block_output = jnp.einsum("hts,hsv->htv", scores, values, precision=highest_precision)
    closing_total = running_decay[:, -1, :]
    carried_over_state = jnp.einsum(
        "gbx,gbi->gxi",
        head_keys * jnp.exp(closing_total[:, None, :] - running_decay),
        values,
        precision=highest_precision,
    )
    incoming_state = carried_in(
        (jnp.exp(closing_total), carried_over_state),
        "ep",
        chain_step,
        (jnp.ones_like(closing_total), jnp.zeros_like(carried_over_state)),
    )[1]
    block_result = within_block_output + jnp.einsum(
        "rsd,rda->rsa", query_rows, incoming_state, precision=highest_precision
    )
    inverse = lax.rsqrt(jnp.mean(block_result * block_result, axis=2, keepdims=True) + eps)
    gated = by_head(jax.nn.silu(out_gate_input.astype(jnp.float32)))
    normed_heads = (block_result * inverse * head_gain * gated).transpose(1, 0, 2)
    head_out = normed_heads.reshape(length, heads_here * head_size).astype(jnp.bfloat16)
    mixed = jnp.dot(
        lax.all_gather(head_out, "tp", axis=1, tiled=True),
        w_mix_out,
        preferred_element_type=jnp.float32,
    )
    return mixed.astype(jnp.bfloat16)


def experts_layer(moe_input, moe_gain, routes, route_weight, w_exp_gate, w_exp_up, w_exp_down):
    row_count = moe_input.shape[0]
    expert_count = lax.axis_size("ep")
    capacity = 5 * row_count * TOP_K // (4 * expert_count)
    token_rows = moe_input.astype(jnp.float32)
    inverse = lax.rsqrt(jnp.mean(token_rows * token_rows, axis=1, keepdims=True) + eps)
    normed = (token_rows * inverse * moe_gain).astype(jnp.bfloat16)
    flat_ids = routes.reshape(-1)
    pair_count = flat_ids.shape[0]
    one_hot = (flat_ids[:, None] == jnp.arange(expert_count, dtype=jnp.int32)[None, :]).astype(
        jnp.int32
    )
    earlier_count = jnp.cumsum(one_hot, axis=0) - one_hot
    ranks = jnp.sum(earlier_count * one_hot, axis=1)
    slot_ids = flat_ids * capacity + ranks
    owners = (
        jnp.zeros((expert_count * capacity,), jnp.int32)
        .at[slot_ids]
        .set(jnp.arange(pair_count, dtype=jnp.int32) // TOP_K)
    )
    filled = (
        jnp.zeros((expert_count * capacity,), jnp.bfloat16)
        .at[slot_ids]
        .set(jnp.ones((pair_count,), jnp.bfloat16))
    )
    outgoing = normed[owners] * filled[:, None]
    w_gate = w_exp_gate[0]
    w_up = w_exp_up[0]
    w_down = w_exp_down[0]
    width = normed.shape[1] // lax.axis_size("tp")
    own_slice = lax.dynamic_slice_in_dim(outgoing, lax.axis_index("tp") * width, width, 1)
    arrived = lax.all_to_all(own_slice, "ep", split_axis=0, concat_axis=0, tiled=True)
    portion = lax.all_gather(arrived, "tp", axis=1, tiled=True)
    gate_sum = jnp.dot(portion, w_gate, preferred_element_type=jnp.float32)
    up_sum = jnp.dot(portion, w_up, preferred_element_type=jnp.float32)
    hidden = (jax.nn.silu(gate_sum) * up_sum).astype(jnp.bfloat16)
    partial_value = jnp.dot(hidden, w_down, preferred_element_type=jnp.float32)
    summed = lax.psum_scatter(
        partial_value.astype(jnp.bfloat16), "tp", scatter_dimension=1, tiled=True
    )
    returned = lax.all_to_all(summed, "ep", split_axis=0, concat_axis=0, tiled=True)
    picked = returned[slot_ids].astype(jnp.float32).reshape(row_count, TOP_K, returned.shape[1])
    combined = jnp.sum(picked * route_weight[:, :, None], axis=1)
    return combined.astype(jnp.bfloat16)


def body(
    mix_query,
    forget_input,
    mix_value,
    out_gate_input,
    decay_shift,
    forget_floor,
    head_gain,
    w_mix_out,
    moe_input,
    moe_gain,
    routes,
    route_weight,
    w_exp_gate,
    w_exp_up,
    w_exp_down,
):
    mixed = token_mixer(
        mix_query,
        forget_input,
        mix_value,
        out_gate_input,
        decay_shift,
        forget_floor,
        head_gain,
        w_mix_out,
    )
    moe_out = experts_layer(
        moe_input, moe_gain, routes, route_weight, w_exp_gate, w_exp_up, w_exp_down
    )
    return (mixed, moe_out)


def solution(mesh):
    placed = (
        P("ep", "tp"),
        P("ep", "tp"),
        P("ep", "tp"),
        P("ep", "tp"),
        P("ep", "tp"),
        P("tp"),
        P(),
        P(None, "tp"),
        P("ep", None),
        P(),
        P("ep", None),
        P("ep", None),
        P("ep", None, "tp"),
        P("ep", None, "tp"),
        P("ep", "tp", None),
    )
    return jax.shard_map(
        body, mesh=mesh, in_specs=placed, out_specs=(P("ep", "tp"), P("ep", "tp")), check_vma=False
    )
```

profile of v0, /device:TPU:0, one launch (start us, length us, event | category | flops | bytes accessed | tf_op | source)
XLA Modules:
  0.0 189.2 jit_solution(8927491651452208620)
XLA Ops:
  11.0 2.4 %scatter_custom_fusion = s32[640]{0:T(1024)S(1)} fusion(s32[512]{0:T(512)S(1)} %bitcast.123, s32[512]{0:T(512)S(1)} %add_select_fusion, s32[]{:T(128)} %constant.68.clone.1), kind=kCustom, calls=%fused_computation.82 | custom fusion | bytes 2564 | tf_op jit(solution)/shard_map/scatter | solution.py:112
  13.5 1.5 fusion.9
  15.0 1.5 fusion.11
  16.5 4.1 %gather_fusion = bf16[640,2048]{1,0:T(8,128)(2,1)} fusion(bf16[256,2048]{1,0:T(8,128)(2,1)S(1)} %fusion.11, s32[1024]{0:T(1024)S(1)} %pad_clamp_fusion.1), kind=kCustom, calls=%fused_computation | custom fusion | bytes 5245440 | tf_op jit(solution)/shard_map/gather | solution.py:119
  20.6 3.8 %scatter_custom_fusion.1 = bf16[640]{0:T(1024)(128)(2,1)S(1)} fusion(s32[512]{0:T(512)S(1)} %bitcast.124, bf16[512]{0:T(512)(128)(2,1)S(1)} %broadcast.119, bf16[]{:T(256)} %constant.79.clone.1), kind=kCustom, calls=%fused_computation.87 | custom fusion | bytes 1282 | tf_op jit(solution)/shard_map/scatter | solution.py:117
  24.4 1.3 dynamic-slice_multiply_fusion
  25.7 24.9 %all_to_all.24 = bf16[8,80,512]{2,1,0:T(8,128)(2,1)} all-to-all(bf16[8,80,512]{2,1,0:T(8,128)(2,1)S(1)} %bitcast.112), channel_id=1, replica_groups=mesh['ep'=8,'tp'=4] {'ep'}, dimensions={0} | all-to-all | bytes 1310720 | tf_op jit(solution)/shard_map/all_to_all | solution.py:125
  53.9 2.2 %copy.97 = f32[256,4,128]{2,1,0:T(4,128)} copy(f32[256,4,128]{0,2,1:T(8,128)} %bitcast.114) | data formatting | bytes 1048576 | tf_op jit(solution)/shard_map/reshape | solution.py:54
  58.8 2.8 %bitcast_multiply_fusion.2 = (f32[4,256,128]{2,0,1:T(4,128)}, f32[4,256,128]{2,0,1:T(4,128)S(1)}, f32[4,256,128]{2,0,1:T(4,128)S(1)}) fusion(f32[256,4,128]{2,1,0:T(4,128)} %copy.97, f32[4,128,256]{1,2,0:T(8,128)S(1)} %bitcast.110, f32[4,128]{1,0:T(4,128)S(1)} %get-tuple-element.60, f32[256,4,128]{2,1,0:T(4,128)} %copy.91), kind=kLoop, calls=%fused_computation.47 | loop fusion | flops 655360 | bytes 3147776 | tf_op jit(solution)/shard_map/mul | solution.py:61
  61.5 1.3 convolution_convert_fusion.1
  63.1 11.9 %all-gather.8.cloned.1.call-done = bf16[640,2048]{1,0:T(8,128)(2,1)} async-done(((bf16[640,512]{1,0:T(8,128)(2,1)}), bf16[640,2048]{1,0:T(8,128)(2,1)}) %all-gather.8.cloned.1.call-update) | async-done | bytes 2621456 | tf_op jit(solution)/shard_map/all_gather | solution.py:126
  75.0 7.4 %fusion.2 = f32[640,1024]{1,0:T(8,128)} fusion(bf16[640,2048]{1,0:T(8,128)(2,1)} %all-gather.8.cloned.1.call-done, bf16[1,2048,1024]{2,1,0:T(8,128)(2,1)} %param.30), kind=kOutput, calls=%fused_computation.8 | convolution fusion | flops 2684354560 | bytes 9437184 | tf_op jit(solution)/shard_map/dot_general | solution.py:128
  82.3 12.5 %fusion.6 = bf16[640,2048]{1,0:T(8,128)(2,1)} fusion(bf16[1,1024,2048]{2,1,0:T(8,128)(2,1)} %param.31, f32[640,1024]{1,0:T(8,128)} %fusion.2, bf16[640,2048]{1,0:T(8,128)(2,1)} %all-gather.8.cloned.1.call-done, bf16[1,2048,1024]{2,1,0:T(8,128)(2,1)} %param.29), kind=kOutput, calls=%fused_computation.12 | convolution fusion | flops 5373952000 | bytes 16252928 | tf_op jit(solution)/shard_map/dot_general | solution.py:130
  94.9 26.4 %all-gather = bf16[32,1,128]{2,1,0:T(2,128)(2,1)S(1)} all-gather(bf16[4,1,128]{2,1,0:T(2,128)(2,1)S(1)} %copy.102), channel_id=2, replica_groups=mesh['ep'=8,'tp'=4] {'ep'}, dimensions={0}, use_global_device_ids=true | all-gather | bytes 9216 | tf_op jit(solution)/shard_map/all_gather | solution.py:14
  121.6 3.0 %convolution_select_fusion = f32[4,256,256]{2,1,0:T(8,128)} fusion(f32[4,256,128]{2,0,1:T(4,128)} %get-tuple-element.57, pred[256,256]{1,0:T(8,128)(4,1)S(1)} %iota_compare_fusion, f32[4,256,128]{2,0,1:T(4,128)S(1)} %get-tuple-element.59), kind=kOutput, calls=%fused_computation.19 | convolution fusion | flops 402915328 | bytes 2162688 | tf_op jit(solution)/shard_map/htk,hsk->hts/dot_general | solution.py:60
  125.4 2.2 %multiply_reduce_fusion.1 = (f32[4,256]{1,0:T(4,128)S(1)}, f32[4,256,128]{1,2,0:T(8,128)S(1)}) fusion(f32[4,256,128]{1,2,0:T(8,128)S(1)} %fusion.36, f32[4,256,256]{2,1,0:T(8,128)} %convolution_select_fusion, bf16[256,512]{1,0:T(8,128)(2,1)} %param.19), kind=kOutput, calls=%fused_computation.54 | convolution fusion | flops 403045376 | bytes 2363392 | tf_op jit(solution)/shard_map/hts,hsv->htv/dot_general | solution.py:65
  128.4 25.2 %reduce-scatter.2.cloned.1.call-done = bf16[640,512]{1,0:T(8,128)(2,1)} async-done(((bf16[640,2048]{1,0:T(8,128)(2,1)}), bf16[640,512]{1,0:T(8,128)(2,1)}) %reduce-scatter.2.cloned.1.call-update) | async-done | bytes 655376 | tf_op jit(solution)/shard_map/reduce_scatter | solution.py:131
  153.7 5.5 %all-to-all-start.1 = ((bf16[8,80,512]{2,1,0:T(8,128)(2,1)}), bf16[8,80,512]{2,1,0:T(8,128)(2,1)S(1)}, u32[]{:S(2)}, u32[]{:S(2)}) async-start(bf16[8,80,512]{2,1,0:T(8,128)(2,1)} %bitcast.119), calls=%async_computation.2 | async-start | bytes 1310720 | tf_op jit(solution)/shard_map/all_to_all | solution.py:134
  159.3 13.1 %all-gather.6.cloned.1.call-done = bf16[256,2048]{0,1:T(8,128)(2,1)} async-done(((bf16[256,512]{0,1:T(8,128)(2,1)}), bf16[256,2048]{0,1:T(8,128)(2,1)}) %all-gather.6.cloned.1.call-update) | async-done | bytes 1048592 | tf_op jit(solution)/shard_map/all_gather | solution.py:87
  172.4 2.7 %convolution_convert_fusion = bf16[256,512]{1,0:T(8,128)(2,1)} fusion(bf16[256,2048]{0,1:T(8,128)(2,1)} %all-gather.6.cloned.1.call-done, bf16[2048,512]{1,0:T(8,128)(2,1)S(1)} %copy-done), kind=kOutput, calls=%fused_computation.21 | convolution fusion | flops 537001984 | bytes 3407872 | tf_op jit(solution)/shard_map/dot_general | solution.py:86
  175.0 1.3 all-to-all-done.1
  176.3 2.6 %gather_fusion.1 = bf16[512,512]{1,0:T(8,128)(2,1)} fusion(bf16[640,512]{1,0:T(8,128)(2,1)S(1)} %bitcast.108, s32[1024]{0:T(1024)S(1)} %pad_clamp_fusion), kind=kCustom, calls=%fused_computation.1 | custom fusion | bytes 1050624 | tf_op jit(solution)/shard_map/gather | solution.py:135
  178.9 1.7 reshape.158
  180.6 2.1 %multiply_reduce_fusion = bf16[256,512]{1,0:T(8,128)(2,1)} fusion(f32[256,2,512]{2,1,0:T(2,128)S(1)} %reshape.158, f32[256,2]{1,0:T(8,128)S(1)} %copy.110), kind=kLoop, calls=%fused_computation.23 | loop fusion | flops 393216 | bytes 1312768 | tf_op jit(solution)/shard_map/reduce_sum | solution.py:136
  (69 shorter events, 12.1 us)
Async XLA Ops:
  7.2 165.2 %copy-start = (bf16[2048,512]{1,0:T(8,128)(2,1)S(1)}, bf16[2048,512]{1,0:T(8,128)(2,1)}, u32[]{:S(2)}) copy-start(bf16[2048,512]{1,0:T(8,128)(2,1)} %param.24) | copy-start | bytes 6291460
  7.2 67.8 %all-gather.8.cloned.1.call-start = ((), (), s32[]{:S(2)}) async-start(), calls=%async_computation.4 | async-start | bytes 3276800 | tf_op jit(solution)/shard_map/all_gather | solution.py:126
  20.6 30.0 %copy-start.2 = (bf16[256,512]{1,0:T(8,128)(2,1)S(1)}, bf16[256,512]{1,0:T(8,128)(2,1)}, u32[]{:S(2)}) copy-start(bf16[256,512]{1,0:T(8,128)(2,1)} %param.18) | copy-start | bytes 786436
  20.6 30.2 %copy-start.4 = (f32[512]{0:T(512)S(1)}, f32[512]{0:T(512)}, u32[]{:S(2)}) copy-start(f32[512]{0:T(512)} %param.22) | copy-start | bytes 6148
  20.6 30.2 %copy-start.5 = (f32[256,4]{0,1:T(4,128)S(1)}, f32[256,4]{0,1:T(4,128)}, u32[]{:S(2)}) copy-start(f32[256,4]{0,1:T(4,128)} %param.21) | copy-start | bytes 12292
  50.6 74.1 %all-gather.10.cloned.1.call-start = ((), (), s32[]{:S(2)}) async-start(), calls=%async_computation.6 | async-start | bytes 1179648 | tf_op jit(solution)/shard_map/all_gather | solution.py:14
  53.9 7.6 %copy-start.1 = (bf16[256,512]{1,0:T(8,128)(2,1)S(1)}, bf16[256,512]{1,0:T(8,128)(2,1)}, u32[]{:S(2)}) copy-start(bf16[256,512]{1,0:T(8,128)(2,1)} %param.19) | copy-start | bytes 786436
  62.9 90.8 %reduce-scatter.2.cloned.1.call-start = ((), (), s32[]{:S(2)}) async-start(), calls=%async_computation.5 | async-start | bytes 3276800 | tf_op jit(solution)/shard_map/reduce_scatter | solution.py:131
  94.8 26.5 %copy-start.3 = (bf16[256,512]{1,0:T(8,128)(2,1)S(1)}, bf16[256,512]{1,0:T(8,128)(2,1)}, u32[]{:S(2)}) copy-start(bf16[256,512]{1,0:T(8,128)(2,1)} %param.20) | copy-start | bytes 786436
  94.8 77.6 %all-gather.6.cloned.1.call-start = ((), (), s32[]{:S(2)}) async-start(), calls=%async_computation.3 | async-start | bytes 1310720 | tf_op jit(solution)/shard_map/all_gather | solution.py:87
  124.7 2.9 %copy-start.7 = (f32[128]{0:T(128)S(1)}, f32[128]{0:T(128)}, u32[]{:S(2)}) copy-start(f32[128]{0:T(128)} %param.23) | copy-start | bytes 1540
  125.4 33.8 %copy-start.6 = (f32[256,2]{0,1:T(2,128)S(1)}, f32[256,2]{0,1:T(2,128)}, u32[]{:S(2)}) copy-start(f32[256,2]{0,1:T(2,128)} %param.28) | copy-start | bytes 6148
  153.7 22.6 %all-to-all-start.1 = ((bf16[8,80,512]{2,1,0:T(8,128)(2,1)}), bf16[8,80,512]{2,1,0:T(8,128)(2,1)S(1)}, u32[]{:S(2)}, u32[]{:S(2)}) async-start(bf16[8,80,512]{2,1,0:T(8,128)(2,1)} %bitcast.119), calls=%async_computation.2 | async-start | bytes 1310720 | tf_op jit(solution)/shard_map/all_to_all | solution.py:134
Sparse Core Ops, SparseCore 0:
  50.7 24.2 all-gather.7
  77.7 40.3 all-gather.9
  120.5 33.0 reduce-scatter.1
  155.7 16.6 all-gather.5
where the time goes:
time: 190 us; the launch traced here: 189 us
  waiting for transfers between devices  51.5 us (27%)
  blocking collectives  51.3 us (27%)
  matrix products  29.7 us (16%)
  local copies, waits for them, and re-layouts  22.4 us (12%)
  other arithmetic  14.5 us (8%)
  between operations  14 us (7%)
  starting transfers between devices  5.83 us (3%)
    all_gather x1, blocking collectives, carried_in(): lax.all_gather(a.astype(kind), axis)  26.4 us
    reduce_scatter x1, waiting for transfers between devices, experts_layer(): lax.psum_scatter(partial_value.astype(jnp.bfloat16), 'tp', scatter_dimens...  25.2 us
    all_to_all x1, blocking collectives, experts_layer(): lax.all_to_all(own_slice, 'ep', split_axis=0, concat_axis=0, tiled=True)  24.9 us
    all_gather x1, waiting for transfers between devices, token_mixer(): lax.all_gather(head_out, 'tp', axis=1, tiled=True)  13.1 us
    dot_general x1, matrix products, experts_layer(): partial_value = jnp.dot(hidden, w_down, preferred_element_type=jnp.float32)  12.5 us
    all_gather x1, waiting for transfers between devices, experts_layer(): portion = lax.all_gather(arrived, 'tp', axis=1, tiled=True)  11.9 us
    dot_general x1, matrix products, experts_layer(): up_sum = jnp.dot(portion, w_up, preferred_element_type=jnp.float32)  7.36 us
    all_to_all x1, starting transfers between devices, experts_layer(): lax.all_to_all(summed, 'ep', split_axis=0, concat_axis=0, tiled=True)  5.49 us
  transfers between devices with their start and end apart: 5, of which 4 were waited for; matrix products, arithmetic and copies ran while one was open for 22% of the time, Pallas kernels for 0%

commit v1 on v0

--- a/solution.py
+++ b/solution.py
@@ -123,7 +123,23 @@
     width = normed.shape[1] // lax.axis_size("tp")
     own_slice = lax.dynamic_slice_in_dim(outgoing, lax.axis_index("tp") * width, width, 1)
     arrived = lax.all_to_all(own_slice, "ep", split_axis=0, concat_axis=0, tiled=True)
-    portion = lax.all_gather(arrived, "tp", axis=1, tiled=True)
+
+    def find_masks(block_in):
+        n_axis = lax.axis_size("tp")
+        x_new = sorted(((dev_j, (dev_j + 1) % n_axis) for dev_j in range(n_axis)))
+        vec_out = block_in
+        stack_in = [vec_out]
+        num = 1
+        while num < n_axis:
+            vec_out = lax.ppermute(vec_out, "tp", x_new)
+            stack_in.insert(0, vec_out)
+            num = num + 1
+        t_next = jnp.concatenate(stack_in, axis=1)
+        item_now = lax.axis_index("tp")
+        all_rows = item_now + 1
+        return jnp.roll(t_next, shift=all_rows * block_in.shape[1], axis=1)
+
+    portion = find_masks(arrived)
     gate_sum = jnp.dot(portion, w_gate, preferred_element_type=jnp.float32)
     up_sum = jnp.dot(portion, w_up, preferred_element_type=jnp.float32)
     hidden = (jax.nn.silu(gate_sum) * up_sum).astype(jnp.bfloat16)

time: 190 us -> 182 us (0.958)
  waiting for transfers between devices: 51.5 us -> 28.2 us
  local copies, waits for them, and re-layouts: 22.4 us -> 34.5 us
  starting transfers between devices: 5.83 us -> 9.96 us
  matrix products: 29.7 us -> 26.4 us
  between operations: 14 us -> 15.9 us
    reduce_scatter x1, waiting for transfers between devices: 25.2 us -> 0.03 us  [experts_layer(): lax.psum_scatter(partial_value.astype(jnp.bfloat16), 'tp', scatter_dimens...]
    ppermute x0 -> x3, waiting for transfers between devices: none -> 15.2 us  [find_masks(): vec_out = lax.ppermute(vec_out, 'tp', x_new)]
    all_gather x1 -> x0, waiting for transfers between devices: 11.9 us -> none  [experts_layer(): portion = lax.all_gather(arrived, 'tp', axis=1, tiled=True)]
    unnamed x22 -> x33, local copies, waits for them, and re-layouts: 2.49 us -> 13.7 us
    all_to_all x1, starting transfers between devices: 5.49 us -> 9.65 us  [experts_layer(): lax.all_to_all(summed, 'ep', split_axis=0, concat_axis=0, tiled=True)]
    dot_general x1, matrix products: 7.36 us -> 4.47 us  [experts_layer(): gate_sum = jnp.dot(portion, w_gate, preferred_element_type=jnp.float32)]
  transfers between devices with their start and end apart: 5 -> 7, of which waited for: 4 -> 5; matrix products, arithmetic and copies ran while one was open for 22% -> 27% of each run, Pallas kernels for 0% -> 0%
where the time goes in v1:
time: 182 us; the launch traced here: 181 us
  blocking collectives  51 us (28%)
  local copies, waits for them, and re-layouts  34.5 us (19%)
  waiting for transfers between devices  28.2 us (15%)
  matrix products  26.4 us (15%)
  between operations  15.9 us (9%)
  other arithmetic  15 us (8%)
  starting transfers between devices  9.96 us (5%)
    all_gather x1, blocking collectives, carried_in(): lax.all_gather(a.astype(kind), axis)  26.3 us
    all_to_all x1, blocking collectives, experts_layer(): lax.all_to_all(own_slice, 'ep', split_axis=0, concat_axis=0, tiled=True)  24.7 us
    ppermute x3, waiting for transfers between devices, find_masks(): vec_out = lax.ppermute(vec_out, 'tp', x_new)  15.2 us
    unnamed x33, local copies, waits for them, and re-layouts  13.7 us
    dot_general x1, matrix products, experts_layer(): partial_value = jnp.dot(hidden, w_down, preferred_element_type=jnp.float32)  12.2 us
    all_gather x1, waiting for transfers between devices, token_mixer(): lax.all_gather(head_out, 'tp', axis=1, tiled=True)  11.9 us
    all_to_all x1, starting transfers between devices, experts_layer(): lax.all_to_all(summed, 'ep', split_axis=0, concat_axis=0, tiled=True)  9.65 us
    dot_general x1, matrix products, experts_layer(): gate_sum = jnp.dot(portion, w_gate, preferred_element_type=jnp.float32)  4.47 us
  transfers between devices with their start and end apart: 7, of which 5 were waited for; matrix products, arithmetic and copies ran while one was open for 27% of the time, Pallas kernels for 0%

profile of v1, /device:TPU:0, one launch (start us, length us, event | category | flops | bytes accessed | tf_op | source)
XLA Modules:
  0.0 181.1 jit_solution(4565839561469484421)
XLA Ops:
  11.8 2.4 %scatter_custom_fusion = s32[640]{0:T(1024)S(1)} fusion(s32[512]{0:T(512)S(1)} %bitcast.123, s32[512]{0:T(512)S(1)} %add_select_fusion, s32[]{:T(128)} %constant.87.clone.1), kind=kCustom, calls=%fused_computation.92 | custom fusion | bytes 2564 | tf_op jit(solution)/shard_map/scatter | solution.py:112
  14.3 1.5 fusion.11
  15.8 1.5 fusion.13
  17.4 4.1 %gather_fusion = bf16[640,2048]{1,0:T(8,128)(2,1)} fusion(bf16[256,2048]{1,0:T(8,128)(2,1)S(1)} %fusion.13, s32[1024]{0:T(1024)S(1)} %pad_clamp_fusion.1), kind=kCustom, calls=%fused_computation | custom fusion | bytes 5245440 | tf_op jit(solution)/shard_map/gather | solution.py:119
  21.5 3.8 %scatter_custom_fusion.1 = bf16[640]{0:T(1024)(128)(2,1)S(1)} fusion(s32[512]{0:T(512)S(1)} %bitcast.124, bf16[512]{0:T(512)(128)(2,1)S(1)} %broadcast.123, bf16[]{:T(256)} %constant.98.clone.1), kind=kCustom, calls=%fused_computation.97 | custom fusion | bytes 1282 | tf_op jit(solution)/shard_map/scatter | solution.py:117
  26.5 24.7 %all_to_all.24 = bf16[8,80,512]{2,1,0:T(8,128)(2,1)S(1)} all-to-all(bf16[8,80,512]{2,1,0:T(8,128)(2,1)S(1)} %bitcast.112), channel_id=1, replica_groups=mesh['ep'=8,'tp'=4] {'ep'}, dimensions={0} | all-to-all | bytes 1310720 | tf_op jit(solution)/shard_map/all_to_all | solution.py:125
  54.5 6.9 %collective-permute-done = bf16[640,512]{1,0:T(8,128)(2,1)} collective-permute-done((bf16[640,512]{1,0:T(8,128)(2,1)S(1)}, bf16[640,512]{1,0:T(8,128)(2,1)}, u32[]{:S(2)}, u32[]{:S(2)}) %collective-permute-start) | collective-permute-done | bytes 655392 | tf_op jit(solution)/shard_map/ppermute | solution.py:134
  63.5 8.2 %collective-permute-done.1 = bf16[640,512]{1,0:T(8,128)(2,1)} collective-permute-done((bf16[640,512]{1,0:T(8,128)(2,1)}, bf16[640,512]{1,0:T(8,128)(2,1)}, u32[]{:S(2)}, u32[]{:S(2)}) %collective-permute-start.1) | collective-permute-done | bytes 655392 | tf_op jit(solution)/shard_map/ppermute | solution.py:134
  71.7 2.0 %copy.97 = f32[256,4,128]{2,1,0:T(4,128)} copy(f32[256,4,128]{0,2,1:T(8,128)} %bitcast.114) | data formatting | bytes 1048576 | tf_op jit(solution)/shard_map/reshape | solution.py:54
  73.8 1.8 copy.90
  75.6 1.9 %copy.91 = f32[256,4,128]{2,1,0:T(4,128)} copy(bf16[256,4,128]{0,2,1:T(8,128)(2,1)} %bitcast.118) | data formatting | bytes 786432 | tf_op jit(solution)/shard_map/transpose | solution.py:54
  77.5 2.8 %bitcast_multiply_fusion.2 = (f32[4,256,128]{2,0,1:T(4,128)}, f32[4,256,128]{2,0,1:T(4,128)S(1)}, f32[4,256,128]{2,0,1:T(4,128)}) fusion(f32[256,4,128]{2,1,0:T(4,128)} %copy.97, f32[4,128,256]{1,2,0:T(8,128)S(1)} %bitcast.111, f32[4,128]{1,0:T(4,128)S(1)} %get-tuple-element.60, f32[256,4,128]{2,1,0:T(4,128)} %copy.91), kind=kLoop, calls=%fused_computation.49 | loop fusion | flops 655360 | bytes 3147776 | tf_op jit(solution)/shard_map/mul | solution.py:61
  89.5 2.3 %copy-done.4 = bf16[640,4096]{1,0:T(8,128)(2,1)} copy-done((bf16[640,4096]{1,0:T(8,128)(2,1)}, bf16[640,4096]{1,0:T(8,128)(2,1)S(1)}, u32[]{:S(2)}) %copy-start.4) | copy-done | bytes 5242904
  91.8 4.5 %fusion.4 = f32[640,1024]{1,0:T(8,128)} fusion(bf16[1,2048,1024]{2,1,0:T(8,128)(2,1)S(1)} %copy-done.9, bf16[640,4096]{1,0:T(8,128)(2,1)S(1)} %constant_dynamic-update-slice_fusion, s32[]{:T(128)S(6)} %select_n.53), kind=kOutput, calls=%fused_computation.10 | convolution fusion | flops 2684354560 | bytes 9437188 | tf_op jit(solution)/shard_map/dot_general | solution.py:143
  96.2 12.2 %fusion.6 = bf16[640,2048]{1,0:T(8,128)(2,1)} fusion(bf16[1,1024,2048]{2,1,0:T(8,128)(2,1)} %param.31, f32[640,1024]{1,0:T(8,128)} %fusion.4, bf16[1,2048,1024]{2,1,0:T(8,128)(2,1)} %param.30, bf16[640,4096]{1,0:T(8,128)(2,1)} %copy-done.4, s32[]{:T(128)S(6)} %select_n.53), kind=kOutput, calls=%fused_computation.12 | convolution fusion | flops 5373952000 | bytes 16252932 | tf_op jit(solution)/shard_map/dot_general | solution.py:146
  108.5 26.3 %all-gather = bf16[32,1,128]{2,1,0:T(2,128)(2,1)S(1)} all-gather(bf16[4,1,128]{2,1,0:T(2,128)(2,1)S(1)} %copy.102), channel_id=2, replica_groups=mesh['ep'=8,'tp'=4] {'ep'}, dimensions={0}, use_global_device_ids=true | all-gather | bytes 9216 | tf_op jit(solution)/shard_map/all_gather | solution.py:14
  135.2 3.1 %convolution_select_fusion = f32[4,256,256]{2,1,0:T(8,128)} fusion(f32[4,256,128]{2,0,1:T(4,128)} %get-tuple-element.57, pred[256,256]{1,0:T(8,128)(4,1)S(1)} %iota_compare_fusion, f32[4,256,128]{2,0,1:T(4,128)S(1)} %copy-done.1), kind=kOutput, calls=%fused_computation.21 | convolution fusion | flops 402915328 | bytes 2162688 | tf_op jit(solution)/shard_map/htk,hsk->hts/dot_general | solution.py:60
  139.0 2.0 %multiply_reduce_fusion.1 = (f32[4,256]{1,0:T(4,128)S(1)}, f32[4,256,128]{1,2,0:T(8,128)S(1)}) fusion(f32[4,256,128]{1,2,0:T(8,128)S(1)} %fusion.42, f32[4,256,256]{2,1,0:T(8,128)} %convolution_select_fusion, bf16[256,512]{1,0:T(8,128)(2,1)} %param.19), kind=kOutput, calls=%fused_computation.56 | convolution fusion | flops 403045376 | bytes 2363392 | tf_op jit(solution)/shard_map/hts,hsv->htv/dot_general | solution.py:65
  141.9 9.7 %all-to-all-start.1 = ((bf16[8,80,512]{2,1,0:T(8,128)(2,1)}), bf16[8,80,512]{2,1,0:T(8,128)(2,1)S(1)}, u32[]{:S(2)}, u32[]{:S(2)}) async-start(bf16[8,80,512]{2,1,0:T(8,128)(2,1)} %bitcast.119), calls=%async_computation.2 | async-start | bytes 1310720 | tf_op jit(solution)/shard_map/all_to_all | solution.py:150
  151.7 11.9 %all-gather.5.cloned.1.call-done = bf16[256,2048]{0,1:T(8,128)(2,1)} async-done(((bf16[256,512]{0,1:T(8,128)(2,1)}), bf16[256,2048]{0,1:T(8,128)(2,1)}) %all-gather.5.cloned.1.call-update) | async-done | bytes 1048592 | tf_op jit(solution)/shard_map/all_gather | solution.py:87
  163.6 2.7 %convolution_convert_fusion = bf16[256,512]{1,0:T(8,128)(2,1)} fusion(bf16[256,2048]{0,1:T(8,128)(2,1)} %all-gather.5.cloned.1.call-done, bf16[2048,512]{1,0:T(8,128)(2,1)S(1)} %copy-done), kind=kOutput, calls=%fused_computation.23 | convolution fusion | flops 537001984 | bytes 3407872 | tf_op jit(solution)/shard_map/dot_general | solution.py:86
  167.3 2.6 %gather_fusion.1 = bf16[512,512]{1,0:T(8,128)(2,1)} fusion(bf16[640,512]{1,0:T(8,128)(2,1)S(1)} %bitcast.106, s32[1024]{0:T(1024)S(1)} %pad_clamp_fusion), kind=kCustom, calls=%fused_computation.1 | custom fusion | bytes 1050624 | tf_op jit(solution)/shard_map/gather | solution.py:151
  169.9 1.7 reshape.158
  171.6 2.1 %multiply_reduce_fusion = bf16[256,512]{1,0:T(8,128)(2,1)} fusion(f32[256,2,512]{2,1,0:T(2,128)S(1)} %reshape.158, f32[256,2]{1,0:T(8,128)S(1)} %copy.110), kind=kLoop, calls=%fused_computation.25 | loop fusion | flops 393216 | bytes 1312768 | tf_op jit(solution)/shard_map/reduce_sum | solution.py:152
  (84 shorter events, 22.6 us)
Async XLA Ops:
  8.0 155.6 %copy-start = (bf16[2048,512]{1,0:T(8,128)(2,1)S(1)}, bf16[2048,512]{1,0:T(8,128)(2,1)}, u32[]{:S(2)}) copy-start(bf16[2048,512]{1,0:T(8,128)(2,1)} %param.24) | copy-start | bytes 6291460
  8.0 130.3 %all-gather.7.cloned.1.call-start = ((), (), s32[]{:S(2)}) async-start(), calls=%async_computation.5 | async-start | bytes 1179648 | tf_op jit(solution)/shard_map/all_gather | solution.py:14
  17.3 35.0 %copy-start.5 = (f32[512]{0:T(512)S(1)}, f32[512]{0:T(512)}, u32[]{:S(2)}) copy-start(f32[512]{0:T(512)} %param.22) | copy-start | bytes 6148
  17.4 35.0 %copy-start.6 = (f32[256,4]{0,1:T(4,128)S(1)}, f32[256,4]{0,1:T(4,128)}, u32[]{:S(2)}) copy-start(f32[256,4]{0,1:T(4,128)} %param.21) | copy-start | bytes 12292
  51.3 10.1 %collective-permute-start = (bf16[640,512]{1,0:T(8,128)(2,1)S(1)}, bf16[640,512]{1,0:T(8,128)(2,1)}, u32[]{:S(2)}, u32[]{:S(2)}) collective-permute-start(bf16[640,512]{1,0:T(8,128)(2,1)S(1)} %bitcast.107), channel_id=1, source_target_pairs={{0,1},{1,2},{2,3},{3,0},{4,5},{5,6},{6,7},{7,4},{8,9},{9,10},{10,1... | collective-permute-start | bytes 1966088 | tf_op jit(solution)/shard_map/ppermute | solution.py:134
  61.4 10.3 %collective-permute-start.1 = (bf16[640,512]{1,0:T(8,128)(2,1)}, bf16[640,512]{1,0:T(8,128)(2,1)}, u32[]{:S(2)}, u32[]{:S(2)}) collective-permute-start(bf16[640,512]{1,0:T(8,128)(2,1)} %collective-permute-done), channel_id=1, source_target_pairs={{0,1},{1,2},{2,3},{3,0},{4,5},{5,6},{6,7},{7,4},{8,9},{9,10},{10,1... | collective-permute-start | bytes 1966088 | tf_op jit(solution)/shard_map/ppermute | solution.py:134
  62.9 17.4 %copy-start.2 = (bf16[256,512]{1,0:T(8,128)(2,1)S(1)}, bf16[256,512]{1,0:T(8,128)(2,1)}, u32[]{:S(2)}) copy-start(bf16[256,512]{1,0:T(8,128)(2,1)} %param.19) | copy-start | bytes 786436
  71.7 10.3 %collective-permute-start.2 = (bf16[640,512]{1,0:T(8,128)(2,1)}, bf16[640,512]{1,0:T(8,128)(2,1)}, u32[]{:S(2)}, u32[]{:S(2)}) collective-permute-start(bf16[640,512]{1,0:T(8,128)(2,1)} %collective-permute-done.1), channel_id=1, source_target_pairs={{0,1},{1,2},{2,3},{3,0},{4,5},{5,6},{6,7},{7,4},{8,9},{9,10},{10,1... | collective-permute-start | bytes 1966088 | tf_op jit(solution)/shard_map/ppermute | solution.py:134
  81.6 60.3 %reduce-scatter.2.cloned.1.call-start = ((), (), s32[]{:S(2)}) async-start(), calls=%async_computation.4 | async-start | bytes 3276800 | tf_op jit(solution)/shard_map/reduce_scatter | solution.py:147
  84.4 7.4 %copy-start.9 = (bf16[1,2048,1024]{2,1,0:T(8,128)(2,1)S(1)}, bf16[1,2048,1024]{2,1,0:T(8,128)(2,1)}, u32[]{:S(2)}) copy-start(bf16[1,2048,1024]{2,1,0:T(8,128)(2,1)} %param.29) | copy-start | bytes 12582916
  89.4 2.3 %copy-start.4 = (bf16[640,4096]{1,0:T(8,128)(2,1)}, bf16[640,4096]{1,0:T(8,128)(2,1)S(1)}, u32[]{:S(2)}) copy-start(bf16[640,4096]{1,0:T(8,128)(2,1)S(1)} %constant_dynamic-update-slice_fusion) | copy-start | bytes 15728644
  96.2 38.6 %copy-start.3 = (bf16[256,512]{1,0:T(8,128)(2,1)S(1)}, bf16[256,512]{1,0:T(8,128)(2,1)}, u32[]{:S(2)}) copy-start(bf16[256,512]{1,0:T(8,128)(2,1)} %param.20) | copy-start | bytes 786436
  108.5 26.7 %copy-start.1 = (f32[4,256,128]{2,0,1:T(4,128)S(1)}, f32[4,256,128]{2,0,1:T(4,128)}, u32[]{:S(2)}) copy-start(f32[4,256,128]{2,0,1:T(4,128)} %get-tuple-element.59) | copy-start | bytes 1572868
  108.5 55.1 %all-gather.5.cloned.1.call-start = ((), (), s32[]{:S(2)}) async-start(), calls=%async_computation.3 | async-start | bytes 1310720 | tf_op jit(solution)/shard_map/all_gather | solution.py:87
  138.3 2.7 %copy-start.8 = (f32[128]{0:T(128)S(1)}, f32[128]{0:T(128)}, u32[]{:S(2)}) copy-start(f32[128]{0:T(128)} %param.23) | copy-start | bytes 1540
  138.3 13.2 %copy-start.7 = (f32[256,2]{0,1:T(2,128)S(1)}, f32[256,2]{0,1:T(2,128)}, u32[]{:S(2)}) copy-start(f32[256,2]{0,1:T(2,128)} %param.28) | copy-start | bytes 6148
  141.9 25.4 %all-to-all-start.1 = ((bf16[8,80,512]{2,1,0:T(8,128)(2,1)}), bf16[8,80,512]{2,1,0:T(8,128)(2,1)S(1)}, u32[]{:S(2)}, u32[]{:S(2)}) async-start(bf16[8,80,512]{2,1,0:T(8,128)(2,1)} %bitcast.119), calls=%async_computation.2 | async-start | bytes 1310720 | tf_op jit(solution)/shard_map/all_to_all | solution.py:150
Sparse Core Ops, SparseCore 0:
  81.8 39.2 all-gather.6
Sparse Core Ops, SparseCore 1:
  108.6 33.1 reduce-scatter.1
  143.7 19.9 all-gather.4
